TPU v7x, 32 devices: a whole 2x2x4 slice. The times are simulated.
32 devices in a mesh: ep: 8 (over z, y), tp: 4 (over x, core).
Axes of the slice: x: 2, y: 2, z: 4, core: 2. Of those that a mesh axis runs over, the one named last changes fastest.
Arguments:
- tokens: bfloat16 [1792, 2048], P('ep'), may hold values from -6 to 6
- cotangent: bfloat16 [1792, 2048], P('ep'), may hold values from -6 to 6
- routes: int32 [1792, 2], P('ep'), may hold values from 0 to 7, all different within a row; in each aligned block of 224 rows (0 to 223, 224 to 447, ...) at most 112 rows name the same one
- gate_weights: float32 [1792, 2], P('ep'), may hold values from 0.2 to 1
- w_gate: bfloat16 [8, 2048, 1792], P('ep', None, 'tp'), may hold values from -0.125 to 0.125
- w_up: bfloat16 [8, 2048, 1792], P('ep', None, 'tp'), may hold values from -0.125 to 0.125
- w_down: bfloat16 [8, 1792, 2048], P('ep', 'tp'), may hold values from -0.125 to 0.125
Outputs:
- token_grad: bfloat16 [1792, 2048], P('ep', 'tp')
- score_grad: float32 [1792, 2], P('ep')
- gate_grad: bfloat16 [8, 2048, 1792], P('ep', None, 'tp')
- up_grad: bfloat16 [8, 2048, 1792], P('ep', None, 'tp')
- down_grad: bfloat16 [8, 1792, 2048], P('ep', 'tp')
- row_norms: float32 [2048], replicated
Inputs may be any that keep to these rules, and one draw needn't show every extreme that they name: `routes`: within the rows of one device, no expert is named by more than 112 of the pairs; some expert is named by exactly 112 of them in some blocks. The 2 experts of a token differ.
All inputs are finite; a program needn't handle non-finite values.
Results may differ from a plain program's by a relative error of at most 0.014.
Values may be sent and summed in bfloat16 or wider, within the bound.
A program may use at most 128 MiB of HBM per device.

v0:
```python
import jax
import jax.numpy as jnp
from jax import lax
from jax.sharding import PartitionSpec as P


def slot_places(routes, experts, capacity):
    flat = routes.reshape(-1)
    onehot = (flat[:, None] == jnp.arange(experts, dtype=jnp.int32)[None, :]).astype(jnp.int32)
    before = jnp.cumsum(onehot, axis=0) - onehot
    position = jnp.sum(before * onehot, axis=1)
    return flat * capacity + position


def on_device(tokens, cotangent, routes, gate_weights, w_gate, w_up, w_down):
    experts = lax.axis_size("ep")
    groups = lax.axis_size("tp")
    tok_rows, width = tokens.shape
    top = routes.shape[1]
    capacity = 2 * tok_rows * top // experts
    slots = experts * capacity
    slot_index = slot_places(routes, experts, capacity)
    token_of = jnp.arange(tok_rows * top, dtype=jnp.int32) // top
    slot_token = jnp.full((slots,), tok_rows, jnp.int32).at[slot_index].set(token_of)
    slot_gate = jnp.zeros((slots,), jnp.float32).at[slot_index].set(gate_weights.reshape(-1))
    gate_send = slot_gate.astype(jnp.bfloat16).reshape(experts, capacity)
    quarter = width // groups
    offset = lax.axis_index("tp") * quarter
    tok_part = lax.dynamic_slice_in_dim(tokens, offset, quarter, 1)
    cot_part = lax.dynamic_slice_in_dim(cotangent, offset, quarter, 1)
    token_send = jnp.take(tok_part, slot_token, axis=0, mode="fill", fill_value=0).reshape(
        experts, capacity, quarter
    )
    cot_send = jnp.take(cot_part, slot_token, axis=0, mode="fill", fill_value=0).reshape(
        experts, capacity, quarter
    )
    part_rows, part_cot, gate_rows = (
        lax.all_to_all(token_send, "ep", split_axis=0, concat_axis=0, tiled=True),
        lax.all_to_all(cot_send, "ep", split_axis=0, concat_axis=0, tiled=True),
        lax.all_to_all(gate_send, "ep", split_axis=0, concat_axis=0, tiled=True),
    )
    token_rows, cot_rows = (
        lax.all_gather(part_rows, "tp", axis=2, tiled=True),
        lax.all_gather(part_cot, "tp", axis=2, tiled=True),
    )
    x_rows = token_rows.reshape(slots, width)
    c_rows = cot_rows.reshape(slots, width)
    scale = gate_rows.reshape(slots, 1).astype(jnp.float32)
    wg = w_gate[0]
    wu = w_up[0]
    wd = w_down[0]
    inner = (((1,), (1,)), ((), ()))
    outer = (((0,), (0,)), ((), ()))
    pre_gate = jnp.dot(x_rows, wg, preferred_element_type=jnp.float32)
    pre_up = jnp.dot(x_rows, wu, preferred_element_type=jnp.float32)
    sig = jax.nn.sigmoid(pre_gate)
    act = pre_gate * sig
    hidden = (act * pre_up).astype(jnp.bfloat16)
    back = lax.dot_general(c_rows, wd, inner, preferred_element_type=jnp.float32)
    score_part = jnp.sum(hidden.astype(jnp.float32) * back, axis=1)
    scaled = scale * back
    d_out = (scale * c_rows).astype(jnp.bfloat16)
    d_gate_pre = (scaled * pre_up * sig * (1.0 + pre_gate * (1.0 - sig))).astype(jnp.bfloat16)
    d_up_pre = (scaled * act).astype(jnp.bfloat16)
    grad_down = lax.dot_general(hidden, d_out, outer, preferred_element_type=jnp.float32).astype(
        jnp.bfloat16
    )
    grad_gate = lax.dot_general(
        x_rows, d_gate_pre, outer, preferred_element_type=jnp.float32
    ).astype(jnp.bfloat16)
    grad_up = lax.dot_general(x_rows, d_up_pre, outer, preferred_element_type=jnp.float32).astype(
        jnp.bfloat16
    )
    partial_value = lax.dot_general(d_gate_pre, wg, inner, preferred_element_type=jnp.float32)
    partial_value = partial_value + lax.dot_general(
        d_up_pre, wu, inner, preferred_element_type=jnp.float32
    )
    score_cols = jnp.broadcast_to(score_part[:, None], (slots, groups))
    token_sum, score_sum = (
        lax.psum_scatter(
            partial_value.astype(jnp.bfloat16), "tp", scatter_dimension=1, tiled=True
        ).astype(jnp.float32),
        lax.psum_scatter(
            score_cols.astype(jnp.bfloat16), "tp", scatter_dimension=1, tiled=True
        ).astype(jnp.float32),
    )
    back_rows = token_sum.astype(jnp.bfloat16).reshape(experts, capacity, -1)
    back_scores = score_sum.astype(jnp.bfloat16).reshape(experts, capacity)
    ret_rows, ret_scores = (
        lax.all_to_all(back_rows, "ep", split_axis=0, concat_axis=0, tiled=True),
        lax.all_to_all(back_scores, "ep", split_axis=0, concat_axis=0, tiled=True),
    )
    picked = jnp.take(ret_rows.reshape(slots, -1), slot_index, axis=0).astype(jnp.float32)
    token_grad = jnp.sum(picked.reshape(tok_rows, top, -1), axis=1).astype(jnp.bfloat16)
    score_grad = (
        jnp.take(ret_scores.reshape(slots), slot_index, axis=0)
        .astype(jnp.float32)
        .reshape(tok_rows, top)
    )
    gate_wide = grad_gate.astype(jnp.float32)
    up_wide = grad_up.astype(jnp.float32)
    norm_part = jnp.sum(gate_wide * gate_wide + up_wide * up_wide, axis=1)
    row_norms = lax.psum(norm_part, ("ep", "tp"))
    return (token_grad, score_grad, grad_gate[None], grad_up[None], grad_down[None], row_norms)


def solution(mesh):
    return jax.shard_map(
        on_device,
        mesh=mesh,
        in_specs=(
            P("ep", None),
            P("ep", None),
            P("ep", None),
            P("ep", None),
            P("ep", None, "tp"),
            P("ep", None, "tp"),
            P("ep", "tp", None),
        ),
        out_specs=(
            P("ep", "tp"),
            P("ep", None),
            P("ep", None, "tp"),
            P("ep", None, "tp"),
            P("ep", "tp", None),
            P(),
        ),
        check_vma=False,
    )
```

profile of v0, /device:TPU:0, one launch (start us, length us, event | category | flops | bytes accessed | tf_op | source)
XLA Modules:
  0.0 247.1 jit_solution(540883861882122742)
XLA Ops:
  7.2 0.9 copy.24
  8.4 1.1 reduce-window.6
  10.0 2.9 %scatter_custom_fusion.1 = s32[896]{0:T(1024)S(1)} fusion(s32[448]{0:T(512)S(1)} %bitcast.51, s32[448]{0:T(512)S(1)} %add_select_fusion, s32[]{:T(128)} %constant.75.clone.1), kind=kCustom, calls=%fused_computation.59 | custom fusion | bytes 3588 | tf_op jit(solution)/shard_map/scatter | solution.py:24
  13.0 1.1 constant_dynamic-slice_fusion
  14.1 3.5 %gather_fusion.3 = bf16[896,512]{1,0:T(8,128)(2,1)S(1)} fusion(bf16[224,512]{1,0:T(8,128)(2,1)S(1)} %get-tuple-element.35, s32[1024]{0:T(1024)S(1)} %pad_clamp_fusion.1), kind=kCustom, calls=%fused_computation.1.clone | custom fusion | bytes 1838592 | tf_op jit(solution)/shard_map/jit(_take)/gather | solution.py:31
  17.6 4.0 %gather_fusion.2 = bf16[896,512]{1,0:T(8,128)(2,1)} fusion(bf16[224,512]{1,0:T(8,128)(2,1)S(1)} %get-tuple-element.36, s32[1024]{0:T(1024)S(1)} %pad_clamp_fusion.1), kind=kCustom, calls=%fused_computation.clone | custom fusion | bytes 1838592 | tf_op jit(solution)/shard_map/jit(_take)/gather | solution.py:34
  21.6 2.3 broadcast_select_fusion.1
  23.9 30.6 %all_to_all.35 = bf16[8,112,512]{2,1,0:T(8,128)(2,1)} all-to-all(bf16[8,112,512]{2,1,0:T(8,128)(2,1)S(1)} %bitcast.48), channel_id=1, replica_groups=mesh['ep'=8,'tp'=4] {'ep'}, dimensions={0} | all-to-all | bytes 1835008 | tf_op jit(solution)/shard_map/all_to_all | solution.py:38
  54.6 26.3 %all_to_all.36 = bf16[8,112,512]{2,1,0:T(8,128)(2,1)} all-to-all(bf16[8,112,512]{2,1,0:T(8,128)(2,1)S(1)} %bitcast.47), channel_id=1, replica_groups=mesh['ep'=8,'tp'=4] {'ep'}, dimensions={0} | all-to-all | bytes 1835008 | tf_op jit(solution)/shard_map/all_to_all | solution.py:39
  81.3 2.9 %scatter_custom_fusion = f32[896]{0:T(1024)S(1)} fusion(s32[448]{0:T(512)S(1)} %bitcast.52, f32[448]{0:T(512)S(1)} %reshape.171, f32[]{:T(128)} %constant.71.clone.1), kind=kCustom, calls=%fused_computation.61 | custom fusion | bytes 3588 | tf_op jit(solution)/shard_map/scatter | solution.py:25
  84.3 9.5 %all_to_all.37 = bf16[8,1,112]{2,1,0:T(2,128)(2,1)S(1)} all-to-all(bf16[8,1,112]{2,1,0:T(2,128)(2,1)S(1)} %all_to_all.28), channel_id=1, replica_groups=mesh['ep'=8,'tp'=4] {'ep'}, dimensions={0} | all-to-all | bytes 3584 | tf_op jit(solution)/shard_map/all_to_all | solution.py:40
  94.0 6.0 %fusion.6 = f32[896,448]{0,1:T(8,128)} fusion(bf16[896,2048]{1,0:T(8,128)(2,1)} %bitcast.54, bf16[1,2048,448]{1,2,0:T(8,128)(2,1)S(1)} %copy-done), kind=kOutput, calls=%fused_computation.17 | convolution fusion | flops 1644167168 | bytes 7110656 | tf_op jit(solution)/shard_map/dot_general | solution.py:54
  100.0 3.2 %fusion.9 = f32[896,448]{0,1:T(8,128)} fusion(bf16[896,2048]{1,0:T(8,128)(2,1)S(1)} %bitcast.56, bf16[1,2048,448]{1,2,0:T(8,128)(2,1)S(1)} %copy-done.5), kind=kOutput, calls=%fused_computation.20 | convolution fusion | flops 1644167168 | bytes 7110656 | tf_op jit(solution)/shard_map/dot_general | solution.py:55
  103.2 14.7 %all-gather.3.cloned.1.call-done = bf16[8,112,2048]{2,1,0:T(8,128)(2,1)} async-done(((bf16[8,112,512]{2,1,0:T(8,128)(2,1)}), bf16[8,112,2048]{2,1,0:T(8,128)(2,1)}) %all-gather.3.cloned.1.call-update) | async-done | bytes 3670032 | tf_op jit(solution)/shard_map/all_gather | solution.py:44
  117.9 7.1 %multiply_reduce_fusion = (bf16[896]{0:T(1024)(128)(2,1)S(1)}, bf16[896,448]{0,1:T(8,128)(2,1)}, bf16[896,448]{0,1:T(8,128)(2,1)S(1)}, bf16[896,448]{0,1:T(8,128)(2,1)S(1)}) fusion(f32[896,448]{0,1:T(8,128)} %fusion.9, f32[896,448]{0,1:T(8,128)} %fusion.6, f32[896]{0:T(1024)S(1)} %reshape.134, bf16[896,2048]{1,0:T(8,128)(2,1)} %bitcast.58, ...), kind=kOutput, calls=%fused_computation.24 | convolution fusion | flops 1651793024 | bytes 11130112 | tf_op jit(solution)/shard_map/dot_general | solution.py:59
  125.1 2.1 fusion.4
  127.2 4.2 %add_convert_fusion = bf16[896,2048]{1,0:T(8,128)(2,1)} fusion(f32[896,2048]{1,0:T(8,128)S(1)} %fusion.4, bf16[896,448]{0,1:T(8,128)(2,1)S(1)} %get-tuple-element.30, bf16[1,2048,448]{1,2,0:T(8,128)(2,1)S(1)} %copy-done.6), kind=kOutput, calls=%fused_computation.7 | convolution fusion | flops 1647837184 | bytes 13647872 | tf_op jit(solution)/shard_map/dot_general | solution.py:75
  132.7 6.0 %all-reduce.1 = bf16[896,4]{0,1:T(4,128)(2,1)S(1)} all-reduce(bf16[896,4]{0,1:T(4,128)(2,1)S(1)} %broadcast_in_dim.53), channel_id=3, replica_groups=mesh['ep'=8,'tp'=4] {'tp'}, use_global_device_ids=true, to_apply=%region_8.10.clone | all-reduce | flops 3584 | bytes 14336
  138.7 0.7 dynamic-slice_reduce_fusion
  139.4 0.7 all_to_all.29
  140.1 5.7 %all-to-all-start.4 = ((bf16[8,1,112]{2,1,0:T(2,128)(2,1)}), bf16[8,1,112]{2,1,0:T(2,128)(2,1)S(1)}, u32[]{:S(2)}, u32[]{:S(2)}) async-start(bf16[8,1,112]{2,1,0:T(2,128)(2,1)} %all_to_all.29), calls=%async_computation.5 | async-start | bytes 8192 | tf_op jit(solution)/shard_map/all_to_all | solution.py:91
  145.9 6.3 %all-to-all-done.4 = bf16[8,1,112]{2,1,0:T(2,128)(2,1)S(1)} async-done(((bf16[8,1,112]{2,1,0:T(2,128)(2,1)}), bf16[8,1,112]{2,1,0:T(2,128)(2,1)S(1)}, u32[]{:S(2)}, u32[]{:S(2)}) %all-to-all-start.4) | async-done | bytes 1824 | tf_op jit(solution)/shard_map/all_to_all | solution.py:91
  152.2 20.5 %reduce-scatter.2.cloned.1.call-done = bf16[896,512]{1,0:T(8,128)(2,1)} async-done(((bf16[896,2048]{1,0:T(8,128)(2,1)}), bf16[896,512]{1,0:T(8,128)(2,1)}) %reduce-scatter.2.cloned.1.call-update) | async-done | bytes 917520 | tf_op jit(solution)/shard_map/reduce_scatter | solution.py:80
  172.7 5.5 %all-to-all-start.3 = ((bf16[8,112,512]{2,1,0:T(8,128)(2,1)}), bf16[8,112,512]{2,1,0:T(8,128)(2,1)S(1)}, u32[]{:S(2)}, u32[]{:S(2)}) async-start(bf16[8,112,512]{2,1,0:T(8,128)(2,1)} %bitcast.49), calls=%async_computation.4 | async-start | bytes 1835008 | tf_op jit(solution)/shard_map/all_to_all | solution.py:90
  178.2 4.5 %convolution_convert_fusion.1 = bf16[2048,448]{0,1:T(8,128)(2,1)S(1)} fusion(bf16[896,448]{0,1:T(8,128)(2,1)} %copy-done.9, bf16[896,2048]{1,0:T(8,128)(2,1)} %bitcast.55), kind=kOutput, calls=%fused_computation.13 | convolution fusion | flops 1645084672 | bytes 6307840 | tf_op jit(solution)/shard_map/dot_general | solution.py:68
  182.8 3.4 %add_reduce_fusion = (f32[2048]{0:T(1024)S(1)}, bf16[2048,448]{0,1:T(8,128)(2,1)}) fusion(bf16[2048,448]{0,1:T(8,128)(2,1)S(1)} %convolution_convert_fusion.1, bf16[896,448]{0,1:T(8,128)(2,1)S(1)} %copy-done.11, bf16[896,2048]{1,0:T(8,128)(2,1)S(1)} %bitcast.57), kind=kOutput, calls=%fused_computation.9 | convolution fusion | flops 1650587648 | bytes 8151040 | tf_op jit(solution)/shard_map/dot_general | solution.py:71
  186.2 40.5 %psum.7 = f32[2048]{0:T(1024)} all-reduce(f32[2048]{0:T(1024)S(1)} %get-tuple-element.33), channel_id=1, replica_groups=mesh['ep'=8,'tp'=4] {'ep','tp'}, use_global_device_ids=true, to_apply=%region_10.12 | all-reduce | flops 2048 | bytes 16384 | tf_op jit(solution)/shard_map/psum | solution.py:103
  226.7 5.7 %fusion.3 = bf16[1,448,2048]{2,1,0:T(8,128)(2,1)} fusion(bf16[896,448]{0,1:T(8,128)(2,1)} %get-tuple-element.28, bf16[896,2048]{1,0:T(8,128)(2,1)} %bitcast.59, f32[896]{0:T(1024)S(1)} %reshape.134), kind=kOutput, calls=%fused_computation.14 | convolution fusion | flops 1650589696 | bytes 6311424 | tf_op jit(solution)/shard_map/dot_general | solution.py:65
  232.5 3.2 %gather_fusion.1 = bf16[448]{0:T(512)(128)(2,1)S(1)} fusion(bf16[896]{0:T(1024)(128)(2,1)S(1)} %reshape.132, s32[1024]{0:T(1024)S(1)} %pad_clamp_fusion), kind=kCustom, calls=%fused_computation.3 | custom fusion | bytes 3584 | tf_op jit(solution)/shard_map/jit(_take)/gather | solution.py:96
  235.9 0.7 copy.29
  236.5 2.1 gather_fusion
  238.8 1.8 fusion.14
  (62 shorter events, 3.2 us)
Async XLA Ops:
  7.2 86.8 %copy-start = (bf16[1,2048,448]{1,2,0:T(8,128)(2,1)S(1)}, bf16[1,2048,448]{1,2,0:T(8,128)(2,1)}, u32[]{:S(2)}) copy-start(bf16[1,2048,448]{1,2,0:T(8,128)(2,1)} %param.13) | copy-start | bytes 5505028
  7.2 86.7 %all-gather.5.cloned.1.call-start = ((), (), s32[]{:S(2)}) async-start(), calls=%async_computation.7 | async-start | bytes 4587520 | tf_op jit(solution)/shard_map/all_gather | solution.py:43
  23.9 30.7 %copy-start.1 = (bf16[896,512]{1,0:T(8,128)(2,1)S(1)}, bf16[896,512]{1,0:T(8,128)(2,1)}, u32[]{:S(2)}) copy-start(bf16[896,512]{1,0:T(8,128)(2,1)} %get-tuple-element.31) | copy-start | bytes 2752516
  54.5 26.5 %copy-start.2 = (f32[224,2]{0,1:T(2,128)S(1)}, f32[224,2]{0,1:T(2,128)}, u32[]{:S(2)}) copy-start(f32[224,2]{0,1:T(2,128)} %param.12) | copy-start | bytes 5380
  54.5 63.4 %all-gather.3.cloned.1.call-start = ((), (), s32[]{:S(2)}) async-start(), calls=%async_computation.6 | async-start | bytes 4587520 | tf_op jit(solution)/shard_map/all_gather | solution.py:44
  80.9 91.7 %reduce-scatter.2.cloned.1.call-start = ((), (), s32[]{:S(2)}) async-start(), calls=%async_computation.8 | async-start | bytes 4587520 | tf_op jit(solution)/shard_map/reduce_scatter | solution.py:80
  93.9 6.0 %copy-start.3 = (bf16[8,112,2048]{2,1,0:T(8,128)(2,1)S(1)}, bf16[8,112,2048]{2,1,0:T(8,128)(2,1)}, u32[]{:S(2)}) copy-start(bf16[8,112,2048]{2,1,0:T(8,128)(2,1)} %all-gather.5.cloned.1.call-done) | copy-start | bytes 11010052
  93.9 6.0 %copy-start.5 = (bf16[1,2048,448]{1,2,0:T(8,128)(2,1)S(1)}, bf16[1,2048,448]{1,2,0:T(8,128)(2,1)}, u32[]{:S(2)}) copy-start(bf16[1,2048,448]{1,2,0:T(8,128)(2,1)} %param.14) | copy-start | bytes 5505028
  125.0 2.1 copy-start.9
  125.0 2.1 copy-start.10
  125.0 2.2 copy-start.6
  131.5 0.7 copy-start.8
  140.1 12.1 %all-to-all-start.4 = ((bf16[8,1,112]{2,1,0:T(2,128)(2,1)}), bf16[8,1,112]{2,1,0:T(2,128)(2,1)S(1)}, u32[]{:S(2)}, u32[]{:S(2)}) async-start(bf16[8,1,112]{2,1,0:T(2,128)(2,1)} %all_to_all.29), calls=%async_computation.5 | async-start | bytes 8192 | tf_op jit(solution)/shard_map/all_to_all | solution.py:91
  172.7 63.9 %all-to-all-start.3 = ((bf16[8,112,512]{2,1,0:T(8,128)(2,1)}), bf16[8,112,512]{2,1,0:T(8,128)(2,1)S(1)}, u32[]{:S(2)}, u32[]{:S(2)}) async-start(bf16[8,112,512]{2,1,0:T(8,128)(2,1)} %bitcast.49), calls=%async_computation.4 | async-start | bytes 1835008 | tf_op jit(solution)/shard_map/all_to_all | solution.py:90
  178.2 4.5 %copy-start.4 = (bf16[8,112,2048]{2,1,0:T(8,128)(2,1)S(1)}, bf16[8,112,2048]{2,1,0:T(8,128)(2,1)}, u32[]{:S(2)}) copy-start(bf16[8,112,2048]{2,1,0:T(8,128)(2,1)} %all-gather.5.cloned.1.call-done) | copy-start | bytes 11010052
  178.2 4.5 %copy-start.11 = (bf16[896,448]{0,1:T(8,128)(2,1)S(1)}, bf16[896,448]{0,1:T(8,128)(2,1)}, u32[]{:S(2)}) copy-start(bf16[896,448]{0,1:T(8,128)(2,1)} %copy-done.10) | copy-start | bytes 2408452
  182.7 3.4 %copy-start.7 = (bf16[2048,448]{0,1:T(8,128)(2,1)}, bf16[2048,448]{0,1:T(8,128)(2,1)S(1)}, u32[]{:S(2)}) copy-start(bf16[2048,448]{0,1:T(8,128)(2,1)S(1)} %convolution_convert_fusion.1) | copy-start | bytes 5505028
Sparse Core Ops, SparseCore 0:
  54.7 30.1 all-gather.4
  86.4 31.4 all-gather.2
  131.6 41.0 reduce-scatter.1
where the time goes:
time: 248 us; the launch traced here: 247 us
  blocking collectives  113 us (46%)
  waiting for transfers between devices  41.6 us (17%)
  matrix products  36.3 us (15%)
  local copies, waits for them, and re-layouts  25.4 us (10%)
  between operations  14.1 us (6%)
  starting transfers between devices  11.3 us (5%)
  other arithmetic  5.52 us (2%)
    psum x1, blocking collectives, on_device(): row_norms = lax.psum(norm_part, ('ep', 'tp'))  40.5 us
    all_to_all x1, blocking collectives, on_device(): lax.all_to_all(token_send, 'ep', split_axis=0, concat_axis=0, tiled=True)  30.6 us
    all_to_all x1, blocking collectives, on_device(): lax.all_to_all(cot_send, 'ep', split_axis=0, concat_axis=0, tiled=True)  26.3 us
    reduce_scatter x1, waiting for transfers between devices, on_device(): lax.psum_scatter(partial_value.astype(jnp.bfloat16), 'tp', scatter_dimens...  20.5 us
    all_gather x1, waiting for transfers between devices, on_device(): lax.all_gather(part_cot, 'tp', axis=2, tiled=True)  14.7 us
    all_to_all x1, blocking collectives, on_device(): lax.all_to_all(gate_send, 'ep', split_axis=0, concat_axis=0, tiled=True)  9.51 us
    dot_general x1, matrix products, on_device(): lax.dot_general(c_rows, wd, inner, preferred_element_type=jnp.float32)  7.11 us
    all_to_all x1, waiting for transfers between devices, on_device(): lax.all_to_all(back_scores, 'ep', split_axis=0, concat_axis=0, tiled=True)  6.26 us
  transfers between devices with their start and end apart: 5, of which 3 were waited for; matrix products, arithmetic and copies ran while one was open for 13% of the time, Pallas kernels for 0%

commit v1 on v0

v1 whole, which is shorter than its diff:
```python
import functools

import jax
import jax.numpy as jnp
from jax import lax
from jax.experimental import pallas as pl
from jax.experimental.pallas import tpu as pltpu
from jax.sharding import PartitionSpec as P

MESH = pl.DeviceIdType.MESH
F32 = jnp.float32
BF = jnp.bfloat16
INNER = (((1,), (1,)), ((), ()))
OUTER = (((0,), (0,)), ((), ()))
PAD = 16
EXTRA = 2


def kernel(n, sel, tok, cot, wg_h, wu_h, wd_h, ret, gg, gu, gd, nout,
           wg, wu, wd, xs, xd, hid, da_s, du_s, part, ra, rb, sb, fb, nrow, ntp, nep,
           wsem, ssem, rsem, ntps, ntpr, neps, nepr):
    me = lax.axis_index("ep")
    j = lax.axis_index("tp")
    sib = j + 1 - 2 * lax.rem(j, 2)
    far = lax.rem(j + 2, 4)
    farsib = lax.rem(sib + 2, 4)
    cap = xd.shape[2]
    width = xd.shape[3]
    quarter = width // 4
    extra = EXTRA * 128
    rest = quarter - extra
    chunk = 256
    chunks = width // chunk

    weights = [pltpu.make_async_copy(src, dst, wsem.at[k])
               for k, (src, dst) in enumerate(((wg_h, wg), (wu_h, wu), (wd_h, wd)))]
    for w in weights:
        w.start()

    barrier = pltpu.get_barrier_semaphore()

    def greet(s, carry):
        pl.semaphore_signal(barrier, inc=1, device_id=(lax.rem(me + s, n), j), device_id_type=MESH)
        return carry

    lax.fori_loop(1, n, greet, 0)
    for k in range(1, 4):
        pl.semaphore_signal(barrier, inc=1, device_id=(me, lax.rem(j + k, 4)), device_id_type=MESH)

    def cols(q, start, size):
        return pl.ds(pl.multiple_of(q * quarter + start, 128), size)

    def copy(src, dst, kind, send_at, recv_at, dev):
        return pltpu.make_async_remote_copy(
            src_ref=src, dst_ref=dst, send_sem=ssem.at[kind, send_at],
            recv_sem=rsem.at[kind, recv_at], device_id=dev, device_id_type=MESH)

    def direct(e, c):
        out = [copy(xs.at[:, e, :, c[0]], xd.at[:, me, :, c[0]], 0, e, me, (e, j))]
        if extra:
            out.append(copy(xs.at[:, e, :, c[1]], xd.at[:, me, :, c[1]], 1, e, me, (e, j)))
        return out

    own_cols = (cols(j, 0, quarter), cols(far, 0, extra) if extra else None)

    def got_direct(i):
        out = [copy(xd.at[:, i, :, own_cols[0]], xd.at[:, i, :, own_cols[0]], 0, i, i, (i, j))]
        if extra:
            out.append(copy(xd.at[:, i, :, own_cols[1]], xd.at[:, i, :, own_cols[1]], 1, i, i, (i, j)))
        return out

    def sel_rows(a, e, src):
        return jnp.dot(sel[a, e], src[...], preferred_element_type=F32).astype(BF)

    def to_far(i):
        c = cols(j, extra, rest)
        return copy(xd.at[:, i, :, c], xd.at[:, i, :, c], 2, i, i, (me, far))

    def from_far(i):
        c = cols(far, extra, rest)
        return copy(xd.at[:, i, :, c], xd.at[:, i, :, c], 2, i, i, (me, far))

    def to_sib(i, mine):
        a, b = (j, far) if mine else (sib, farsib)
        c = cols(a, 0, quarter)
        out = [copy(xd.at[:, i, :, c], xd.at[:, i, :, c], 3, i, i, (me, sib))]
        if extra:
            c = cols(b, 0, extra)
            out.append(copy(xd.at[:, i, :, c], xd.at[:, i, :, c], 4, i, i, (me, sib)))
        return out

    def rest_sib(i, mine):
        c = cols(far if mine else farsib, extra, rest)
        return copy(xd.at[:, i, :, c], xd.at[:, i, :, c], 5, i, i, (me, sib))

    def step_a(i):
        return [copy(part.at[i, sib], ra.at[i, 0], 6, i, i, (me, sib)),
                copy(part.at[i, farsib], ra.at[i, 1], 7, i, i, (me, sib))]

    def step_b(i):
        return copy(sb.at[i], rb.at[i], 8, i, i, (me, far))

    def step_c(i):
        return copy(fb.at[i], ret.at[me], 9, i, me, (i, j))

    def got_c(i):
        return copy(fb.at[i], ret.at[i], 9, i, i, (i, j))

    def source(s):
        return lax.rem(me - s + n, n)

    def fill(s, carry):
        e = lax.rem(me + s, n)
        xs[0, e] = sel_rows(0, e, tok)
        xs[1, e] = sel_rows(1, e, cot)

        @pl.when(s == 1)
        def _():
            pl.semaphore_wait(barrier, n + 2)

        for c in direct(e, own_cols):
            c.start()
        return carry

    lax.fori_loop(1, n, fill, 0)
    xd[0, me] = sel_rows(0, me, tok)
    xd[1, me] = sel_rows(1, me, cot)
    for w in weights:
        w.wait()

    def f1(s):
        i = source(s)
        for c in got_direct(i):
            c.wait_recv()
        to_far(i).start()
        for c in to_sib(i, True):
            c.start()

    def f2(s):
        i = source(s)
        from_far(i).wait_recv()
        rest_sib(i, True).start()

    def f3(s):
        i = source(s)
        for c in to_sib(i, False):
            c.wait_recv()
        rest_sib(i, False).wait_recv()

    def expert(s):
        i = source(s)
        x = xd[0, i]
        a = jnp.dot(x, wg[...], preferred_element_type=F32)
        u = jnp.dot(x, wu[...], preferred_element_type=F32)
        q = lax.dot_general(xd[1, i], wd[...], INNER, preferred_element_type=F32)
        sig = jax.nn.sigmoid(a)
        act = a * sig
        h = (act * u).astype(BF)
        da = (q * u * sig * (1.0 + a * (1.0 - sig))).astype(BF)
        du = (q * act).astype(BF)
        hid[i] = h
        da_s[i] = da
        du_s[i] = du
        score = jnp.sum(h.astype(F32) * q, axis=1, keepdims=True)
        eye = (lax.broadcasted_iota(jnp.int32, (cap, 128), 0)
               == lax.broadcasted_iota(jnp.int32, (cap, 128), 1))
        row = jnp.sum(jnp.where(eye, score, 0.0), axis=0, keepdims=True)
        tile = jnp.broadcast_to(jnp.concatenate([row] * (quarter // 128), axis=1), (PAD, quarter)).astype(BF)
        for k in range(4):
            c = slice(k * quarter, (k + 1) * quarter)
            p = lax.dot_general(da, wg[c, :], INNER, preferred_element_type=F32)
            p = p + lax.dot_general(du, wu[c, :], INNER, preferred_element_type=F32)
            part[i, k, :cap, :] = p.astype(BF)
            part[i, k, cap:, :] = tile
        for c in step_a(i):
            c.start()

    def do_b(s):
        i = source(s)
        for c in step_a(i):
            c.wait_recv()
        sb[i] = (part[i, far].astype(F32) + ra[i, 1].astype(F32)).astype(BF)
        step_b(i).start()

    def do_c(s):
        i = source(s)
        step_b(i).wait_recv()
        total = (part[i, j].astype(F32) + ra[i, 0].astype(F32) + rb[i].astype(F32)).astype(BF)

        @pl.when(s == 0)
        def _():
            ret[me] = total

        @pl.when(s > 0)
        def _():
            fb[i] = total
            step_c(i).start()

    def main(t, carry):
        @pl.when(t > 0)
        def _():
            f3(t)

        expert(t)

        @pl.when(t == 0)
        def _():
            f1(1)

        @pl.when(t + 2 < n)
        def _():
            f1(t + 2)

        @pl.when(t + 1 < n)
        def _():
            f2(t + 1)

        @pl.when(t > 0)
        def _():
            do_b(t - 1)

        @pl.when(t > 1)
        def _():
            do_c(t - 2)

        return carry

    lax.fori_loop(0, n, main, 0)

    half = lax.broadcasted_iota(jnp.int32, (128, 128), 0) == lax.broadcasted_iota(jnp.int32, (128, 128), 1)

    def wgrad(c, carry):
        at = pl.ds(pl.multiple_of(c * chunk, chunk), chunk)
        rows = n * cap
        x = xd[0, :, :, at].reshape(rows, chunk)
        d = xd[1, :, :, at].reshape(rows, chunk)
        ff = hid.shape[2]
        g = lax.dot_general(x, da_s[...].reshape(rows, ff), OUTER, preferred_element_type=F32).astype(BF)
        gg[at, :] = g
        u = lax.dot_general(x, du_s[...].reshape(rows, ff), OUTER, preferred_element_type=F32).astype(BF)
        gu[at, :] = u
        gd[:, at] = lax.dot_general(hid[...].reshape(rows, ff), d, OUTER, preferred_element_type=F32).astype(BF)
        gw = g.astype(F32)
        uw = u.astype(F32)
        norm = jnp.sum(gw * gw + uw * uw, axis=1, keepdims=True)
        for k in range(chunk // 128):
            nrow[pl.ds(c * (chunk // 128) + k, 1), :] = jnp.sum(
                jnp.where(half, norm[k * 128:(k + 1) * 128], 0.0), axis=0, keepdims=True)

        @pl.when(c == 0)
        def _():
            do_b(n - 1)
            do_c(n - 2)

        @pl.when(c == 2)
        def _():
            do_c(n - 1)

        return carry

    lax.fori_loop(0, chunks, wgrad, 0)

    ntp[j] = nrow[...]

    def tp_copy(k, slot):
        return pltpu.make_async_remote_copy(
            src_ref=ntp.at[slot], dst_ref=ntp.at[slot], send_sem=ntps.at[k], recv_sem=ntpr.at[slot],
            device_id=(me, lax.rem(j + k, 4)), device_id_type=MESH)

    for k in range(1, 4):
        tp_copy(k, j).start()
    for k in range(1, 4):
        tp_copy(k, lax.rem(j + k, 4)).wait_recv()
    nep[me] = ntp[0] + ntp[1] + ntp[2] + ntp[3]

    def ep_copy(s, slot):
        return pltpu.make_async_remote_copy(
            src_ref=nep.at[slot], dst_ref=nep.at[slot], send_sem=neps.at[s], recv_sem=nepr.at[slot],
            device_id=(lax.rem(me + s, n), j), device_id_type=MESH)

    def ep_send(s, carry):
        ep_copy(s, me).start()
        return carry

    lax.fori_loop(1, n, ep_send, 0)

    def drain(s, carry):
        i = source(s)
        for c in direct(i, own_cols) + to_sib(i, True):
            c.wait_send()
        to_far(i).wait_send()
        rest_sib(i, True).wait_send()
        step_c(i).wait_send()
        got_c(i).wait_recv()
        return carry

    lax.fori_loop(1, n, drain, 0)

    def drain_tp(s, carry):
        i = source(s)
        for c in step_a(i):
            c.wait_send()
        step_b(i).wait_send()
        return carry

    lax.fori_loop(0, n, drain_tp, 0)

    def ep_wait(s, carry):
        ep_copy(s, lax.rem(me + s, n)).wait_recv()
        return carry

    lax.fori_loop(1, n, ep_wait, 0)
    nout[...] = lax.fori_loop(1, n, lambda i, acc: acc + nep[i], nep[0])

    def ep_drain(s, carry):
        ep_copy(s, me).wait_send()
        return carry

    lax.fori_loop(1, n, ep_drain, 0)
    for k in range(1, 4):
        tp_copy(k, j).wait_send()


def on_device(n, tokens, cotangent, routes, gate_weights, w_gate, w_up, w_down):
    tok_rows, width = tokens.shape
    top = routes.shape[1]
    ff = w_gate.shape[2]
    capacity = 2 * tok_rows * top // n
    cap = -(-capacity // 16) * 16
    quarter = width // 4
    rows = cap + PAD
    pairs = tok_rows * top

    flat = routes.reshape(-1)
    onehot = (flat[:, None] == jnp.arange(n, dtype=jnp.int32)[None, :]).astype(F32)
    ids = jnp.arange(pairs, dtype=jnp.int32)
    tri = (ids[None, :] < ids[:, None]).astype(BF)
    before = jnp.dot(tri, onehot.astype(BF), preferred_element_type=F32)
    position = jnp.sum(before * onehot, axis=1).astype(jnp.int32)
    slot = (flat * cap + position).reshape(tok_rows, top)
    gates = gate_weights.astype(BF)
    slots = jnp.arange(n * cap, dtype=jnp.int32)[:, None]
    hits = [slots == slot[:, k][None, :] for k in range(top)]
    pick = sum(h.astype(BF) for h in hits)
    pick_g = sum(jnp.where(h, gates[:, k][None, :], jnp.zeros((), BF)) for k, h in enumerate(hits))
    sel = jnp.stack([pick, pick_g]).reshape(2, n, cap, tok_rows)

    vmem = pl.BlockSpec(memory_space=pltpu.VMEM)
    anym = pl.BlockSpec(memory_space=pl.ANY)
    dma = pltpu.SemaphoreType.DMA
    ret, gg, gu, gd, norms = pl.pallas_call(
        functools.partial(kernel, n),
        out_shape=(
            jax.ShapeDtypeStruct((n, rows, quarter), BF),
            jax.ShapeDtypeStruct((width, ff), BF),
            jax.ShapeDtypeStruct((width, ff), BF),
            jax.ShapeDtypeStruct((ff, width), BF),
            jax.ShapeDtypeStruct((width // 128, 128), F32),
        ),
        in_specs=[vmem, vmem, vmem, anym, anym, anym],
        out_specs=(vmem, vmem, vmem, vmem, vmem),
        scratch_shapes=[
            pltpu.VMEM((width, ff), BF), pltpu.VMEM((width, ff), BF), pltpu.VMEM((ff, width), BF),
            pltpu.VMEM((2, n, cap, width), BF), pltpu.VMEM((2, n, cap, width), BF),
            pltpu.VMEM((n, cap, ff), BF), pltpu.VMEM((n, cap, ff), BF), pltpu.VMEM((n, cap, ff), BF),
            pltpu.VMEM((n, 4, rows, quarter), BF),
            pltpu.VMEM((n, 2, rows, quarter), BF),
            pltpu.VMEM((n, rows, quarter), BF), pltpu.VMEM((n, rows, quarter), BF),
            pltpu.VMEM((n, rows, quarter), BF),
            pltpu.VMEM((width // 128, 128), F32),
            pltpu.VMEM((4, width // 128, 128), F32), pltpu.VMEM((n, width // 128, 128), F32),
            dma((3,)), dma((10, n)), dma((10, n)), dma((4,)), dma((4,)), dma((n,)), dma((n,)),
        ],
        compiler_params=pltpu.CompilerParams(
            collective_id=0, has_side_effects=True, vmem_limit_bytes=62 * 1024 * 1024),
    )(sel, tokens, cotangent, w_gate[0], w_up[0], w_down[0])

    back = ret.reshape(n * rows, quarter)
    spot = flat * rows + position
    spots = jnp.arange(n * rows, dtype=jnp.int32)[None, :]
    spot2 = spot.reshape(tok_rows, top)
    comb = sum((spots == spot2[:, k][:, None]).astype(BF) for k in range(top))
    token_grad = jnp.dot(comb, back, preferred_element_type=F32).astype(BF)
    scores = ret[:, cap, :cap].reshape(1, n * cap).astype(F32)
    wanted = slot.reshape(pairs, 1) == jnp.arange(n * cap, dtype=jnp.int32)[None, :]
    score = jnp.sum(jnp.where(wanted, scores, 0.0), axis=1).reshape(tok_rows, top)
    score_grad = score / gates.astype(F32)
    return token_grad, score_grad, gg[None], gu[None], gd[None], norms.reshape(width)


def solution(mesh):
    return jax.shard_map(
        functools.partial(on_device, mesh.shape["ep"]),
        mesh=mesh,
        in_specs=(
            P("ep", None),
            P("ep", None),
            P("ep", None),
            P("ep", None),
            P("ep", None, "tp"),
            P("ep", None, "tp"),
            P("ep", "tp", None),
        ),
        out_specs=(
            P("ep", "tp"),
            P("ep", None),
            P("ep", None, "tp"),
            P("ep", None, "tp"),
            P("ep", "tp", None),
            P(),
        ),
        check_vma=False,
    )
```

time: 248 us -> 147 us (0.59)
  Pallas kernels: 0 us -> 124 us
  blocking collectives: 113 us -> 0 us
  waiting for transfers between devices: 41.6 us -> 0 us
  matrix products: 36.3 us -> 1.36 us
  between operations: 14.1 us -> 0.74 us
  starting transfers between devices: 11.3 us -> 0 us
  local copies, waits for them, and re-layouts: 25.4 us -> 17.5 us
  other arithmetic: 5.52 us -> 2.49 us
    pallas_call x0 -> x1, Pallas kernels: none -> 124 us  [on_device(): pl.pallas_call(functools.partial(kernel, n), out_shape=(jax.ShapeDtypeStr...]
    all_to_all x3 -> x0, blocking collectives: 66.4 us -> none  [the longest x1 30.6 us: on_device(): lax.all_to_all(token_send, 'ep', split_axis=0, concat_axis=0, tiled=True)]
    psum x1 -> x0, blocking collectives: 40.5 us -> none  [on_device(): row_norms = lax.psum(norm_part, ('ep', 'tp'))]
    dot_general x8 -> x2, matrix products: 36.3 us -> 1.36 us  [the longest x1 1.14 us: on_device(): token_grad = jnp.dot(comb, back, preferred_element_type=F32).astype(BF)]
    reduce_scatter x1 -> x0, waiting for transfers between devices: 20.5 us -> none  [on_device(): lax.psum_scatter(partial_value.astype(jnp.bfloat16), 'tp', scatter_dimens...]
    all_gather x2 -> x0, waiting for transfers between devices: 14.7 us -> none  [the longest x1 14.7 us: on_device(): lax.all_gather(part_cot, 'tp', axis=2, tiled=True)]
    unnamed x29 -> x19, local copies, waits for them, and re-layouts: 3.65 us -> 16.8 us
    gather x6 -> x0, local copies, waits for them, and re-layouts: 13.1 us -> none  [the longest x1 3.98 us: on_device(): jnp.take(cot_part, slot_token, axis=0, mode='fill', fill_value=0)]
  transfers between devices with their start and end apart: 5 -> 0, of which waited for: 3 -> 0; matrix products, arithmetic and copies ran while one was open for 13% -> 0% of each run, Pallas kernels for 0% -> 0%
where the time goes in v1:
time: 147 us; the launch traced here: 146 us
  Pallas kernels  124 us (84%)
  local copies, waits for them, and re-layouts  17.5 us (12%)
  other arithmetic  2.49 us (2%)
    pallas_call x1, Pallas kernels, on_device(): pl.pallas_call(functools.partial(kernel, n), out_shape=(jax.ShapeDtypeStr...  124 us
    unnamed x19, local copies, waits for them, and re-layouts  16.8 us

profile of v1, /device:TPU:0, one launch (start us, length us, event | category | flops | bytes accessed | tf_op | source)
XLA Modules:
  0.0 146.3 jit_solution(1748639434973071503)
XLA Ops:
  0.6 0.8 copy.53
  1.5 0.0 copy-start.2
  1.5 0.2 slice_reduce_fusion.1
  1.7 0.9 copy.50
  2.6 0.1 eq.125
  2.7 0.2 fusion
  3.0 0.1 convert_element_type.70
  3.1 0.1 copy.51
  3.2 0.7 multiply_add_fusion.3
  3.9 0.3 fusion.6
  4.2 1.1 pad_maximum_fusion.sel
  5.3 0.0 copy-done.2
  5.3 2.4 %copy.54 = bf16[1,2048,448]{2,1,0:T(8,128)(2,1)} copy(bf16[1,2048,448]{1,2,0:T(8,128)(2,1)S(1)} %copy-done.2) | data formatting | bytes 3670016 | tf_op args[4]
  7.7 3.8 %copy.55 = bf16[1,2048,448]{2,1,0:T(8,128)(2,1)} copy(bf16[1,2048,448]{1,2,0:T(8,128)(2,1)} %param.12) | data formatting | bytes 3670016 | tf_op args[5]
  11.6 124.2 %shard_map.118 = (bf16[8,128,512]{2,1,0:T(8,128)(2,1)}, bf16[2048,448]{1,0:T(8,128)(2,1)}, bf16[2048,448]{1,0:T(8,128)(2,1)}, bf16[448,2048]{1,0:T(8,128)(2,1)}, f32[16,128]{1,0:T(8,128)}) custom-call(bf16[2,8,112,224]{3,2,1,0:T(8,128)(2,1)} %pad_maximum_fusion.sel, bf16[224,2048]{1,0:T(8,128)(2,1)} %tok.1, bf16[224,2048]{1,0:T(8,128)(2,1)} %cot.1, ...), custom_call_target="tpu_custom_call" | custom-call | tf_op jit(solution)/shard_map/pallas_call | solution.py:351
  135.8 0.0 copy-start
  135.8 4.0 %copy.57 = bf16[1,2048,448]{1,2,0:T(8,128)(2,1)} copy(bf16[1,2048,448]{2,1,0:T(8,128)(2,1)} %bitcast.16) | data formatting | bytes 3670016
  139.8 0.0 copy-done
  139.8 0.0 copy-start.4
  139.8 2.3 %copy.58 = bf16[1,2048,448]{1,2,0:T(8,128)(2,1)} copy(bf16[1,2048,448]{2,1,0:T(8,128)(2,1)S(1)} %bitcast.15) | data formatting | bytes 3670016
  142.1 0.0 copy-done.4
  142.1 0.0 copy-start.1
  142.1 0.1 reshape.172
  142.2 0.3 select_reduce_fusion
  142.5 0.1 reshape.170
  142.7 0.7 copy.56
  143.4 1.1 convolution_convert_fusion
  144.5 0.0 copy-done.1
  144.5 0.0 copy-start.3
  144.5 1.2 copy.61
  145.7 0.0 copy-done.3
  145.7 0.6 copy.62
  (6 shorter events, 0.1 us)
Async XLA Ops:
  1.5 3.9 %copy-start.2 = (bf16[1,2048,448]{1,2,0:T(8,128)(2,1)S(1)}, bf16[1,2048,448]{1,2,0:T(8,128)(2,1)}, u32[]{:S(2)}) copy-start(bf16[1,2048,448]{1,2,0:T(8,128)(2,1)} %param.11) | copy-start | bytes 5505028
  135.8 4.0 %copy-start = (bf16[2048,448]{1,0:T(8,128)(2,1)S(1)}, bf16[2048,448]{1,0:T(8,128)(2,1)}, u32[]{:S(2)}) copy-start(bf16[2048,448]{1,0:T(8,128)(2,1)} %get-tuple-element.13) | copy-start | bytes 5505028
  139.8 2.3 %copy-start.4 = (bf16[8,128,512]{2,1,0:T(8,128)(2,1)S(1)}, bf16[8,128,512]{2,1,0:T(8,128)(2,1)}, u32[]{:S(2)}) copy-start(bf16[8,128,512]{2,1,0:T(8,128)(2,1)} %get-tuple-element.11) | copy-start | bytes 3145732
  142.1 2.4 %copy-start.1 = (bf16[448,2048]{1,0:T(8,128)(2,1)S(1)}, bf16[448,2048]{1,0:T(8,128)(2,1)}, u32[]{:S(2)}) copy-start(bf16[448,2048]{1,0:T(8,128)(2,1)} %get-tuple-element.14) | copy-start | bytes 5505028
  144.5 1.2 copy-start.3

commit v2 on v1

--- a/solution.py
+++ b/solution.py
@@ -150,8 +150,8 @@
     def expert(s):
         i = source(s)
         x = xd[0, i]
-        a = jnp.dot(x, wg[...], preferred_element_type=F32)
-        u = jnp.dot(x, wu[...], preferred_element_type=F32)
+        a = lax.dot_general(x, wg[...], INNER, preferred_element_type=F32)
+        u = lax.dot_general(x, wu[...], INNER, preferred_element_type=F32)
         q = lax.dot_general(xd[1, i], wd[...], INNER, preferred_element_type=F32)
         sig = jax.nn.sigmoid(a)
         act = a * sig
@@ -168,8 +168,8 @@
         tile = jnp.broadcast_to(jnp.concatenate([row] * (quarter // 128), axis=1), (PAD, quarter)).astype(BF)
         for k in range(4):
             c = slice(k * quarter, (k + 1) * quarter)
-            p = lax.dot_general(da, wg[c, :], INNER, preferred_element_type=F32)
-            p = p + lax.dot_general(du, wu[c, :], INNER, preferred_element_type=F32)
+            p = jnp.dot(da, wg[:, c], preferred_element_type=F32)
+            p = p + jnp.dot(du, wu[:, c], preferred_element_type=F32)
             part[i, k, :cap, :] = p.astype(BF)
             part[i, k, cap:, :] = tile
         for c in step_a(i):
@@ -226,8 +226,6 @@
         return carry
 
     lax.fori_loop(0, n, main, 0)
-
-    half = lax.broadcasted_iota(jnp.int32, (128, 128), 0) == lax.broadcasted_iota(jnp.int32, (128, 128), 1)
 
     def wgrad(c, carry):
         at = pl.ds(pl.multiple_of(c * chunk, chunk), chunk)
@@ -235,17 +233,16 @@
         x = xd[0, :, :, at].reshape(rows, chunk)
         d = xd[1, :, :, at].reshape(rows, chunk)
         ff = hid.shape[2]
-        g = lax.dot_general(x, da_s[...].reshape(rows, ff), OUTER, preferred_element_type=F32).astype(BF)
-        gg[at, :] = g
-        u = lax.dot_general(x, du_s[...].reshape(rows, ff), OUTER, preferred_element_type=F32).astype(BF)
-        gu[at, :] = u
+        g = lax.dot_general(da_s[...].reshape(rows, ff), x, OUTER, preferred_element_type=F32).astype(BF)
+        gg[:, at] = g
+        u = lax.dot_general(du_s[...].reshape(rows, ff), x, OUTER, preferred_element_type=F32).astype(BF)
+        gu[:, at] = u
         gd[:, at] = lax.dot_general(hid[...].reshape(rows, ff), d, OUTER, preferred_element_type=F32).astype(BF)
         gw = g.astype(F32)
         uw = u.astype(F32)
-        norm = jnp.sum(gw * gw + uw * uw, axis=1, keepdims=True)
+        norm = jnp.sum(gw * gw + uw * uw, axis=0, keepdims=True)
         for k in range(chunk // 128):
-            nrow[pl.ds(c * (chunk // 128) + k, 1), :] = jnp.sum(
-                jnp.where(half, norm[k * 128:(k + 1) * 128], 0.0), axis=0, keepdims=True)
+            nrow[pl.ds(c * (chunk // 128) + k, 1), :] = norm[:, k * 128:(k + 1) * 128]
 
         @pl.when(c == 0)
         def _():
@@ -352,15 +349,15 @@
         functools.partial(kernel, n),
         out_shape=(
             jax.ShapeDtypeStruct((n, rows, quarter), BF),
-            jax.ShapeDtypeStruct((width, ff), BF),
-            jax.ShapeDtypeStruct((width, ff), BF),
+            jax.ShapeDtypeStruct((ff, width), BF),
+            jax.ShapeDtypeStruct((ff, width), BF),
             jax.ShapeDtypeStruct((ff, width), BF),
             jax.ShapeDtypeStruct((width // 128, 128), F32),
         ),
         in_specs=[vmem, vmem, vmem, anym, anym, anym],
         out_specs=(vmem, vmem, vmem, vmem, vmem),
         scratch_shapes=[
-            pltpu.VMEM((width, ff), BF), pltpu.VMEM((width, ff), BF), pltpu.VMEM((ff, width), BF),
+            pltpu.VMEM((ff, width), BF), pltpu.VMEM((ff, width), BF), pltpu.VMEM((ff, width), BF),
             pltpu.VMEM((2, n, cap, width), BF), pltpu.VMEM((2, n, cap, width), BF),
             pltpu.VMEM((n, cap, ff), BF), pltpu.VMEM((n, cap, ff), BF), pltpu.VMEM((n, cap, ff), BF),
             pltpu.VMEM((n, 4, rows, quarter), BF),
@@ -373,7 +370,7 @@
         ],
         compiler_params=pltpu.CompilerParams(
             collective_id=0, has_side_effects=True, vmem_limit_bytes=62 * 1024 * 1024),
-    )(sel, tokens, cotangent, w_gate[0], w_up[0], w_down[0])
+    )(sel, tokens, cotangent, w_gate[0].T, w_up[0].T, w_down[0])
 
     back = ret.reshape(n * rows, quarter)
     spot = flat * rows + position
@@ -385,7 +382,7 @@
     wanted = slot.reshape(pairs, 1) == jnp.arange(n * cap, dtype=jnp.int32)[None, :]
     score = jnp.sum(jnp.where(wanted, scores, 0.0), axis=1).reshape(tok_rows, top)
     score_grad = score / gates.astype(F32)
-    return token_grad, score_grad, gg[None], gu[None], gd[None], norms.reshape(width)
+    return token_grad, score_grad, gg.T[None], gu.T[None], gd[None], norms.reshape(width)
 
 
 def solution(mesh):

time: 147 us -> 140 us (0.952)
  local copies, waits for them, and re-layouts: 17.5 us -> 9.23 us
    unnamed x19 -> x15, local copies, waits for them, and re-layouts: 16.8 us -> 8.44 us
where the time goes in v2:
time: 140 us; the launch traced here: 139 us
  Pallas kernels  123 us (88%)
  local copies, waits for them, and re-layouts  9.23 us (7%)
  other arithmetic  3.21 us (2%)
  matrix products  2.72 us (2%)
    pallas_call x1, Pallas kernels, on_device(): pl.pallas_call(functools.partial(kernel, n), out_shape=(jax.ShapeDtypeStr...  123 us
    unnamed x15, local copies, waits for them, and re-layouts  8.44 us

profile of v2, /device:TPU:0, one launch (start us, length us, event | category | flops | bytes accessed | tf_op | source)
XLA Modules:
  0.0 139.3 jit_solution(9876150358152049104)
XLA Ops:
  0.6 0.8 copy.34
  1.4 0.1 eq.125
  1.6 0.2 fusion
  1.8 0.1 convert_element_type.70
  2.0 0.1 copy.35
  2.1 0.7 multiply_add_fusion.3
  2.8 0.8 copy.37
  3.6 0.2 slice_reduce_fusion.1
  3.8 0.3 fusion.6
  4.1 1.1 pad_maximum_fusion.sel
  5.2 123.5 %shard_map.118 = (bf16[8,128,512]{2,1,0:T(8,128)(2,1)}, bf16[448,2048]{1,0:T(8,128)(2,1)}, bf16[448,2048]{1,0:T(8,128)(2,1)}, bf16[448,2048]{1,0:T(8,128)(2,1)}, f32[16,128]{1,0:T(8,128)}) custom-call(bf16[2,8,112,224]{3,2,1,0:T(8,128)(2,1)} %pad_maximum_fusion.sel, bf16[224,2048]{1,0:T(8,128)(2,1)} %tok.1, bf16[224,2048]{1,0:T(8,128)(2,1)} %cot.1, ...), custom_call_target="tpu_custom_call" | custom-call | tf_op jit(solution)/shard_map/pallas_call | solution.py:348
  128.7 0.0 copy-start.2
  128.7 2.5 %convolution_convert_fusion = bf16[224,512]{1,0:T(8,128)(2,1)} fusion(bf16[1024,512]{1,0:T(8,128)(2,1)} %bitcast.32, s32[224]{0:T(256)S(1)} %bitcast.31, s32[224]{0:T(256)S(1)} %bitcast.30), kind=kOutput, calls=%fused_computation.2 | convolution fusion | flops 236830720 | bytes 1279744 | tf_op jit(solution)/shard_map/dot_general | solution.py:380
  131.2 0.7 convert_reduce_fusion
  131.9 0.1 reshape.172
  132.0 0.3 select_reduce_fusion
  132.3 0.1 reshape.170
  132.5 0.7 copy.38
  133.2 0.0 copy-done.2
  133.2 0.0 copy-start.1
  133.2 1.2 copy.43
  134.4 0.9 copy-done.1
  135.3 0.0 copy-start
  135.3 1.2 copy.44
  136.6 0.9 copy-done
  137.5 0.0 copy-start.3
  137.5 1.2 copy.45
  138.7 0.0 copy-done.3
  138.7 0.6 copy.46
  (5 shorter events, 0.1 us)
Async XLA Ops:
  128.7 4.5 %copy-start.2 = (bf16[448,2048]{1,0:T(8,128)(2,1)S(1)}, bf16[448,2048]{1,0:T(8,128)(2,1)}, u32[]{:S(2)}) copy-start(bf16[448,2048]{1,0:T(8,128)(2,1)} %get-tuple-element.12) | copy-start | bytes 5505028
  133.2 2.2 %copy-start.1 = (bf16[448,2048]{1,0:T(8,128)(2,1)S(1)}, bf16[448,2048]{1,0:T(8,128)(2,1)}, u32[]{:S(2)}) copy-start(bf16[448,2048]{1,0:T(8,128)(2,1)} %get-tuple-element.13) | copy-start | bytes 5505028
  135.3 2.2 %copy-start = (bf16[448,2048]{1,0:T(8,128)(2,1)S(1)}, bf16[448,2048]{1,0:T(8,128)(2,1)}, u32[]{:S(2)}) copy-start(bf16[448,2048]{1,0:T(8,128)(2,1)} %get-tuple-element.14) | copy-start | bytes 5505028
  137.5 1.2 copy-start.3
